TPU v7x, 32 devices: a whole 2x2x4 slice. The times are simulated.
32 devices in a mesh: grp: 2 (over x), tp: 16 (over z, y, core).
Axes of the slice: x: 2, y: 2, z: 4, core: 2. Of those that a mesh axis runs over, the one named last changes fastest.
Arguments:
- tokens: bfloat16 [160, 2048], P('grp', 'tp'), parts along dimension 0, may hold values from -6 to 6
- lengths: int32 [160], P('grp'), parts along dimension 0, may hold values from 1 to 4096, 81920 in all
- cell_memory: float32 [2, 160, 2048, 256], P(None, 'grp', 'tp'), parts along dimension 1, may hold values from -0.6 to 0.6
- key_sums: float32 [2, 160, 2048], P(None, 'grp', 'tp'), parts along dimension 1, may hold values from -3 to 3
- stabilizer: float32 [2, 160, 8], P(None, 'grp'), parts along dimension 1, may hold values from -3 to 1
- norm_gain: bfloat16 [2, 2048], replicated, may hold values from 0.099609375 to 1.8984375
- query_weight: bfloat16 [2, 2048, 2048], P(None, None, 'tp'), may hold values from -0.125 to 0.125
- key_weight: bfloat16 [2, 2048, 2048], P(None, None, 'tp'), may hold values from -0.125 to 0.125
- value_weight: bfloat16 [2, 2048, 2048], P(None, None, 'tp'), may hold values from -0.125 to 0.125
- outgate_weight: bfloat16 [2, 2048, 2048], P(None, None, 'tp'), may hold values from -0.125 to 0.125
- ingate_weight: bfloat16 [2, 2048, 8], replicated, may hold values from -0.125 to 0.125
- forget_weight: bfloat16 [2, 2048, 8], replicated, may hold values from -0.125 to 0.125
- ingate_bias: float32 [2, 8], replicated, may hold values from -3 to 3
- forget_bias: float32 [2, 8], replicated, may hold values from -1 to 4
- forget_slope: float32 [2, 8], replicated, may hold values from -3 to 3
- head_gain: bfloat16 [2, 2048], P(None, 'tp'), may hold values from 0.099609375 to 1.8984375
- output_weight: bfloat16 [2, 2048, 2048], P(None, None, 'tp'), may hold values from -0.125 to 0.125
Outputs:
- new_tokens: bfloat16 [160, 2048], P('grp', 'tp'), parts along dimension 0
- new_memory: float32 [2, 160, 2048, 256], P(None, 'grp', 'tp'), parts along dimension 1
- new_key_sums: float32 [2, 160, 2048], P(None, 'grp', 'tp'), parts along dimension 1
- new_stabilizer: float32 [2, 160, 8], P(None, 'grp'), parts along dimension 1
There are 2 independent parts, one for each index of `grp`. A program takes and returns all parts, laid end to end along the dimension named above; an argument that names none is the same for every part. Nothing has to cross between parts.
Inputs may be any that keep to these rules, and one draw needn't show every extreme that they name: Each part's 80 lengths sum to 81920, and the largest is exactly 4096.
All inputs are finite; a program needn't handle non-finite values.
Results may differ from a plain program's by a relative error of at most 0.018.
Values may be sent and summed in bfloat16 or wider, within the bound.
A program may use at most 128 MiB of HBM per device.

v0:
```python
import jax
import jax.numpy as jnp
from jax import lax
from jax.sharding import PartitionSpec as P

HEADS = 8
HEAD = 256
MAXLEN = 4096
EPS = 1e-05


def from_partner(value, axis, stride):
    mask = 2**stride
    pairs = [(source, source ^ mask) for source in range(lax.axis_size(axis))]
    return lax.ppermute(value, axis, pairs)


def body(
    tokens,
    lengths,
    cell_memory,
    key_sums,
    stabilizer,
    norm_gain,
    query_weight,
    key_weight,
    value_weight,
    outgate_weight,
    ingate_weight,
    forget_weight,
    ingate_bias,
    forget_bias,
    forget_slope,
    head_gain,
    output_weight,
):
    devices = lax.axis_size("tp")
    split_count = devices // HEADS
    own_index = lax.axis_index("tp")
    head_id = own_index // split_count
    onehot = (jnp.arange(HEADS) == head_id).astype(jnp.float32)
    position = lengths.astype(jnp.float32) / MAXLEN
    current = tokens
    memories, sums_list, stabs = ([], [], [])
    for block_id in range(cell_memory.shape[0]):
        gathered_rows = lax.all_gather(current, "tp", axis=1, tiled=True)
        row_float = gathered_rows.astype(jnp.float32)
        normed = (
            row_float
            * lax.rsqrt(jnp.mean(row_float * row_float, axis=-1, keepdims=True) + EPS)
            * norm_gain[block_id].astype(jnp.float32)
        ).astype(jnp.bfloat16)
        queries = jnp.dot(
            normed, query_weight[block_id], preferred_element_type=jnp.float32
        ).astype(jnp.bfloat16)
        key_rows = (
            jnp.dot(normed, key_weight[block_id], preferred_element_type=jnp.float32)
            * HEAD ** (-0.5)
        ).astype(jnp.bfloat16)
        values = jnp.dot(normed, value_weight[block_id], preferred_element_type=jnp.float32).astype(
            jnp.bfloat16
        )
        outgate = jnp.dot(
            normed, outgate_weight[block_id], preferred_element_type=jnp.float32
        ).astype(jnp.bfloat16)
        ingate = (
            jnp.dot(normed, ingate_weight[block_id], preferred_element_type=jnp.float32)
            + ingate_bias[block_id]
        )
        forget = jax.nn.log_sigmoid(
            jnp.dot(normed, forget_weight[block_id], preferred_element_type=jnp.float32)
            + forget_bias[block_id]
            + forget_slope[block_id] * position[:, None]
        )
        stab_new = jnp.maximum(forget + stabilizer[block_id], ingate)
        decays = jnp.exp(forget + stabilizer[block_id] - stab_new)
        in_weight = jnp.exp(ingate - stab_new)
        decay_own = jnp.sum(decays * onehot, axis=1)
        inweight_own = jnp.sum(in_weight * onehot, axis=1)
        sums_new = decay_own[:, None] * key_sums[block_id] + inweight_own[
            :, None
        ] * key_rows.astype(jnp.float32)
        head_pair = jnp.stack((queries, key_rows))
        head_sums = sums_new
        for level in range(split_count.bit_length() - 1):
            partner = from_partner(head_pair, "tp", level)
            upper = own_index // (1 << level) % 2 == 1
            lower_half = jnp.where(upper, partner, head_pair)
            upper_half = jnp.where(upper, head_pair, partner)
            head_pair = jnp.concatenate((lower_half, upper_half), axis=2)
            sums_mate = from_partner(head_sums, "tp", level)
            sums_low = jnp.where(upper, sums_mate, head_sums)
            sums_high = jnp.where(upper, head_sums, sums_mate)
            head_sums = jnp.concatenate((sums_low, sums_high), axis=1)
        head_query = head_pair[0].astype(jnp.float32)
        head_keys = head_pair[1].astype(jnp.float32)
        mem_new = (
            decay_own[:, None, None] * cell_memory[block_id]
            + inweight_own[:, None, None]
            * values.astype(jnp.float32)[:, :, None]
            * head_keys[:, None, :]
        )
        numerator = jnp.einsum("bvk,bk->bv", mem_new, head_query, precision=lax.Precision.HIGHEST)
        denominator = jnp.maximum(jnp.abs(jnp.sum(head_sums * head_query, axis=1)), 1.0)
        hidden = numerator / denominator[:, None]
        gated_out = (
            hidden
            * head_gain[block_id].astype(jnp.float32)
            * jax.nn.sigmoid(outgate.astype(jnp.float32))
        ).astype(jnp.bfloat16)
        out_weight = output_weight[block_id]
        projected = jnp.dot(
            lax.all_gather(gated_out, "tp", axis=1, tiled=True),
            out_weight,
            preferred_element_type=jnp.float32,
        )
        current = (current.astype(jnp.float32) + projected).astype(jnp.bfloat16)
        memories.append(mem_new)
        sums_list.append(sums_new)
        stabs.append(stab_new)
    return (current, jnp.stack(memories), jnp.stack(sums_list), jnp.stack(stabs))


def solution(mesh):
    in_specs = (
        P("grp", "tp"),
        P("grp"),
        P(None, "grp", "tp", None),
        P(None, "grp", "tp"),
        P(None, "grp", None),
        P(),
        P(None, None, "tp"),
        P(None, None, "tp"),
        P(None, None, "tp"),
        P(None, None, "tp"),
        P(),
        P(),
        P(),
        P(),
        P(),
        P(None, "tp"),
        P(None, None, "tp"),
    )
    out_specs = (
        P("grp", "tp"),
        P(None, "grp", "tp", None),
        P(None, "grp", "tp"),
        P(None, "grp", None),
    )
    return jax.shard_map(body, mesh=mesh, in_specs=in_specs, out_specs=out_specs, check_vma=False)
```

profile of v0, /device:TPU:0, one launch (start us, length us, event | category | flops | bytes accessed | tf_op | source)
XLA Modules:
  0.0 133.5 jit_solution(18110746305476406706)
XLA Ops:
  0.7 0.7 convert_multiply_fusion.4
  1.3 0.8 slice_bitcast_fusion
  2.1 0.8 slice_convert_fusion
  2.9 24.3 %all_gather.12 = bf16[80,2048]{1,0:T(8,128)(2,1)S(1)} all-gather(bf16[80,128]{1,0:T(8,128)(2,1)} %param.17), channel_id=1, replica_groups=mesh['grp'=2,'tp'=16] {'tp'}, dimensions={1}, use_global_device_ids=true | all-gather | bytes 348160 | tf_op jit(solution)/shard_map/all_gather | solution.py:46
  27.3 0.8 slice_bitcast_fusion.1
  28.1 1.3 %fusion.38 = bf16[1,80,128]{2,1,0:T(8,128)(2,1)S(1)} fusion(bf16[2,2048,128]{2,1,0:T(8,128)(2,1)} %param.23, bf16[80,2048]{1,0:T(8,128)(2,1)S(1)} %all_gather.12, f32[2048]{0:T(1024)S(1)} %bitcast.144, f32[80]{0:T(128)S(1)} %add_rsqrt_fusion.1), kind=kOutput, calls=%fused_computation.51 | convolution fusion | flops 42608640 | bytes 880960 | tf_op jit(solution)/shard_map/dot_general | solution.py:53
  29.4 1.1 fusion.93
  30.6 1.1 multiply_reduce_fusion.3
  31.7 1.4 %fusion.81 = (f32[80,128]{1,0:T(8,128)S(1)}, bf16[80,128]{1,0:T(8,128)(2,1)S(1)}) fusion(f32[2,80,128]{2,1,0:T(8,128)} %param.20, f32[80]{0:T(128)S(1)} %get-tuple-element.6, f32[80]{0:T(128)S(1)} %get-tuple-element.7, bf16[2,2048,128]{2,1,0:T(8,128)(2,1)} %param.24, bf16[80,2048]{1,0:T(8,128)(2,1)S(1)} %all_gather.12, f32[2048]{0:T(1024)S(1)} %bitcast.147, ...), kind=kOutput, calls=%fused_computation.115 | convolution fusion | flops 42659840 | bytes 963520 | tf_op jit(solution)/shard_map/dot_general | solution.py:57
  33.1 0.4 collective-permute-start
  33.5 0.2 collective-permute-start.1
  33.7 1.3 %fusion.37 = f32[80,128]{1,0:T(8,128)S(1)} fusion(bf16[2,2048,128]{2,1,0:T(8,128)(2,1)} %param.25, f32[80]{0:T(128)S(1)} %get-tuple-element.7, bf16[80,2048]{1,0:T(8,128)(2,1)S(1)} %all_gather.12, f32[2048]{0:T(1024)S(1)} %bitcast.148, f32[80]{0:T(128)S(1)} %add_rsqrt_fusion.1), kind=kOutput, calls=%fused_computation.50 | convolution fusion | flops 42629120 | bytes 901760 | tf_op jit(solution)/shard_map/dot_general | solution.py:60
  35.0 0.7 bitcast_convert_fusion
  36.0 8.7 %fusion.4 = f32[80,1,128]{2,1,0:T(1,128)S(1)} fusion(f32[2,80,128,256]{3,2,1,0:T(8,128)} %param.19, f32[80,256]{1,0:T(8,128)S(1)} %get-tuple-element.19, f32[80,128]{1,0:T(8,128)S(1)} %fusion.37, f32[80]{0:T(128)S(1)} %get-tuple-element.6, bf16[80,256,1]{1,0,2:T(8,128)(2,1)S(1)} %get-tuple-element.18), kind=kOutput, calls=%fused_computation.6 | convolution fusion | flops 39321600 | bytes 10690880 | tf_op jit(solution)/shard_map/bvk,bk->bv/dot_general | solution.py:103
  44.7 0.3 fusion.35
  45.0 18.3 %all_gather.13 = bf16[80,2048]{1,0:T(8,128)(2,1)S(1)} all-gather(bf16[80,128]{1,0:T(8,128)(2,1)S(1)} %fusion.35), channel_id=1, replica_groups=mesh['grp'=2,'tp'=16] {'tp'}, dimensions={1}, use_global_device_ids=true | all-gather | bytes 348160 | tf_op jit(solution)/shard_map/all_gather | solution.py:113
  63.3 0.2 fusion.17
  63.6 19.7 %all_gather.14 = bf16[80,2048]{1,0:T(8,128)(2,1)S(1)} all-gather(bf16[80,128]{1,0:T(8,128)(2,1)S(1)} %fusion.17), channel_id=1, replica_groups=mesh['grp'=2,'tp'=16] {'tp'}, dimensions={1}, use_global_device_ids=true | all-gather | bytes 348160 | tf_op jit(solution)/shard_map/all_gather | solution.py:46
  83.4 0.3 fusion.39
  83.8 0.3 fusion.95
  84.1 0.3 multiply_reduce_fusion.1
  84.4 0.3 fusion.28
  84.7 0.3 fusion.80
  85.0 0.4 collective-permute-start.2
  85.6 0.6 pad_maximum_fusion.1
  86.3 0.6 pad_maximum_fusion.6
  87.1 10.3 %multiply_add_fusion.1 = (f32[1,80,128,256]{3,2,1,0:T(8,128)S(1)}, f32[1,80,128,256]{3,2,1,0:T(8,128)S(1)}) fusion(f32[2,80,128,256]{3,2,1,0:T(8,128)} %param.19, f32[80,256]{1,0:T(8,128)S(1)} %get-tuple-element.19, f32[80,128]{1,0:T(8,128)S(1)} %fusion.37, f32[80]{0:T(128)S(1)} %get-tuple-element.6, f32[80,256]{1,0:T(8,128)S(1)} %get-tuple-element.13, ...), kind=kLoop, calls=%fused_computation.8 | loop fusion | flops 15728640 | bytes 42189440 | tf_op jit(solution)/shard_map/add | solution.py:98
  97.4 8.6 %fusion.1 = f32[80,1,128]{2,1,0:T(1,128)S(1)} fusion(f32[2,80,128,256]{3,2,1,0:T(8,128)} %param.19, f32[80,256]{1,0:T(8,128)S(1)} %get-tuple-element.13, f32[80,128]{1,0:T(8,128)S(1)} %fusion.28, f32[80]{0:T(128)S(1)} %get-tuple-element.4, bf16[80,256,1]{1,0,2:T(8,128)(2,1)S(1)} %get-tuple-element.12), kind=kOutput, calls=%fused_computation.3 | convolution fusion | flops 39321600 | bytes 10690880 | tf_op jit(solution)/shard_map/bvk,bk->bv/dot_general | solution.py:103
  106.0 0.3 fusion.26
  106.3 18.3 %all_gather.15 = bf16[80,2048]{1,0:T(8,128)(2,1)S(1)} all-gather(bf16[80,128]{1,0:T(8,128)(2,1)S(1)} %fusion.26), channel_id=1, replica_groups=mesh['grp'=2,'tp'=16] {'tp'}, dimensions={1}, use_global_device_ids=true | all-gather | bytes 348160 | tf_op jit(solution)/shard_map/all_gather | solution.py:113
  124.6 0.9 fusion.19
  125.5 8.0 %pad_maximum_fusion = f32[2,80,128,256]{3,2,1,0:T(8,128)} fusion(f32[1,80,128,256]{3,2,1,0:T(8,128)S(1)} %get-tuple-element.9, f32[1,80,128,256]{3,2,1,0:T(8,128)S(1)} %get-tuple-element.8), kind=kLoop, calls=%fused_computation | loop fusion | flops 5242880 | bytes 41943040 | tf_op jit(solution)/shard_map/stack | solution.py:121
  (42 shorter events, 0.9 us)
Async XLA Ops:
  27.1 36.2 %copy-start = (bf16[80,128]{1,0:T(8,128)(2,1)S(1)}, bf16[80,128]{1,0:T(8,128)(2,1)}, u32[]{:S(2)}) copy-start(bf16[80,128]{1,0:T(8,128)(2,1)} %param.17) | copy-start | bytes 61444
  29.4 54.0 %copy-start.1 = (bf16[2,2048,128]{2,1,0:T(8,128)(2,1)S(1)}, bf16[2,2048,128]{2,1,0:T(8,128)(2,1)}, u32[]{:S(2)}) copy-start(bf16[2,2048,128]{2,1,0:T(8,128)(2,1)} %param.23) | copy-start | bytes 3145732
  31.6 52.1 %copy-start.7 = (bf16[2,2048,8]{1,2,0:T(8,128)(2,1)S(1)}, bf16[2,2048,8]{1,2,0:T(8,128)(2,1)}, u32[]{:S(2)}) copy-start(bf16[2,2048,8]{1,2,0:T(8,128)(2,1)} %param.28) | copy-start | bytes 196612
  31.6 52.1 %copy-start.9 = (f32[2,80,8]{1,2,0:T(8,128)S(1)}, f32[2,80,8]{1,2,0:T(8,128)}, u32[]{:S(2)}) copy-start(f32[2,80,8]{1,2,0:T(8,128)} %param.21) | copy-start | bytes 15364
  31.7 52.4 %copy-start.8 = (bf16[2,2048,8]{1,2,0:T(8,128)(2,1)S(1)}, bf16[2,2048,8]{1,2,0:T(8,128)(2,1)}, u32[]{:S(2)}) copy-start(bf16[2,2048,8]{1,2,0:T(8,128)(2,1)} %param.27) | copy-start | bytes 196612
  33.1 51.3 %copy-start.2 = (bf16[2,2048,128]{2,1,0:T(8,128)(2,1)S(1)}, bf16[2,2048,128]{2,1,0:T(8,128)(2,1)}, u32[]{:S(2)}) copy-start(bf16[2,2048,128]{2,1,0:T(8,128)(2,1)} %param.25) | copy-start | bytes 3145732
  33.1 2.7 %collective-permute-start = (bf16[2,80,128]{2,1,0:T(8,128)(2,1)S(1)}, bf16[2,80,128]{2,1,0:T(8,128)(2,1)S(1)}, u32[]{:S(2)}, u32[]{:S(2)}) collective-permute-start(bf16[2,80,128]{2,1,0:T(8,128)(2,1)S(1)} %pad_maximum_fusion.4), channel_id=1, source_target_pairs={{0,1},{1,0},{2,3},{3,2},{4,5},{5,4},{6,7},{7,6},{8,9},{9,8},{10,11... | collective-permute-start | bytes 122888 | tf_op jit(solution)/shard_map/ppermute | solution.py:15
  33.5 2.3 %collective-permute-start.1 = (f32[80,128]{1,0:T(8,128)S(1)}, f32[80,128]{1,0:T(8,128)S(1)}, u32[]{:S(2)}, u32[]{:S(2)}) collective-permute-start(f32[80,128]{1,0:T(8,128)S(1)} %get-tuple-element.34), channel_id=1, source_target_pairs={{0,1},{1,0},{2,3},{3,2},{4,5},{5,4},{6,7},{7,6},{8,9},{9,8},{10,11... | collective-permute-start | bytes 122888 | tf_op jit(solution)/shard_map/ppermute | solution.py:15
  35.0 49.7 %copy-start.6 = (f32[2,80,128]{2,1,0:T(8,128)S(1)}, f32[2,80,128]{2,1,0:T(8,128)}, u32[]{:S(2)}) copy-start(f32[2,80,128]{2,1,0:T(8,128)} %param.20) | copy-start | bytes 245764
  35.8 8.9 %copy-start.4 = (bf16[2,2048,128]{2,1,0:T(8,128)(2,1)S(1)}, bf16[2,2048,128]{2,1,0:T(8,128)(2,1)}, u32[]{:S(2)}) copy-start(bf16[2,2048,128]{2,1,0:T(8,128)(2,1)} %param.26) | copy-start | bytes 3145732
  35.8 27.6 %copy-start.5 = (bf16[2,2048,128]{2,1,0:T(8,128)(2,1)S(1)}, bf16[2,2048,128]{2,1,0:T(8,128)(2,1)}, u32[]{:S(2)}) copy-start(bf16[2,2048,128]{2,1,0:T(8,128)(2,1)} %param.33) | copy-start | bytes 3145732
  35.8 48.9 %copy-start.3 = (bf16[2,2048,128]{2,1,0:T(8,128)(2,1)S(1)}, bf16[2,2048,128]{2,1,0:T(8,128)(2,1)}, u32[]{:S(2)}) copy-start(bf16[2,2048,128]{2,1,0:T(8,128)(2,1)} %param.24) | copy-start | bytes 3145732
  85.0 1.8 %collective-permute-start.2 = (bf16[2,80,128]{2,1,0:T(8,128)(2,1)S(1)}, bf16[2,80,128]{2,1,0:T(8,128)(2,1)S(1)}, u32[]{:S(2)}, u32[]{:S(2)}) collective-permute-start(bf16[2,80,128]{2,1,0:T(8,128)(2,1)S(1)} %pad_maximum_fusion.5), channel_id=1, source_target_pairs={{0,1},{1,0},{2,3},{3,2},{4,5},{5,4},{6,7},{7,6},{8,9},{9,8},{10,11... | collective-permute-start | bytes 122888 | tf_op jit(solution)/shard_map/ppermute | solution.py:15
  85.5 1.4 %collective-permute-start.3 = (f32[80,128]{1,0:T(8,128)S(1)}, f32[80,128]{1,0:T(8,128)S(1)}, u32[]{:S(2)}, u32[]{:S(2)}) collective-permute-start(f32[80,128]{1,0:T(8,128)S(1)} %get-tuple-element.36), channel_id=1, source_target_pairs={{0,1},{1,0},{2,3},{3,2},{4,5},{5,4},{6,7},{7,6},{8,9},{9,8},{10,11... | collective-permute-start | bytes 122888 | tf_op jit(solution)/shard_map/ppermute | solution.py:15
where the time goes:
time: 134 us; the launch traced here: 133 us
  blocking collectives  80.6 us (60%)
  matrix products  26.8 us (20%)
  other arithmetic  22.4 us (17%)
  local copies, waits for them, and re-layouts  1.58 us (1%)
    all_gather x2, blocking collectives, body(): gathered_rows = lax.all_gather(current, 'tp', axis=1, tiled=True)  43.9 us
    all_gather x2, blocking collectives, body(): lax.all_gather(gated_out, 'tp', axis=1, tiled=True)  36.7 us
    dot_general x2, matrix products, body(): jnp.einsum('bvk,bk->bv', mem_new, head_query, precision=lax.Precision.HIG...  17.2 us
    add x1, other arithmetic, body(): decay_own[:, None, None] * cell_memory[block_id]  10.3 us
    another operation x1, other arithmetic, body(): jnp.stack(memories)  8 us
  transfers between devices with their start and end apart: 4, of which 0 were waited for; matrix products, arithmetic and copies ran while one was open for 3% of the time, Pallas kernels for 0%

commit v1 on v0

--- a/solution.py
+++ b/solution.py
@@ -43,7 +43,12 @@
     current = tokens
     memories, sums_list, stabs = ([], [], [])
     for block_id in range(cell_memory.shape[0]):
-        gathered_rows = lax.all_gather(current, "tp", axis=1, tiled=True)
+
+        def plan_halves(shard_in, pos_dim):
+            new = jnp.concatenate(lax.all_gather(shard_in, "tp"), pos_dim)
+            return new
+
+        gathered_rows = plan_halves(current, 1)
         row_float = gathered_rows.astype(jnp.float32)
         normed = (
             row_float

time: 134 us -> 134 us (level)
  transfers between devices with their start and end apart: 4 -> 4, of which waited for: 0 -> 0; matrix products, arithmetic and copies ran while one was open for 3% -> 2% of each run, Pallas kernels for 0% -> 0%
where the time goes in v1:
time: 134 us; the launch traced here: 133 us
  blocking collectives  80.6 us (60%)
  matrix products  26 us (19%)
  other arithmetic  23.1 us (17%)
  local copies, waits for them, and re-layouts  1.57 us (1%)
    all_gather x2, blocking collectives, plan_halves(): new = jnp.concatenate(lax.all_gather(shard_in, 'tp'), pos_dim)  43.9 us
    all_gather x2, blocking collectives, body(): lax.all_gather(gated_out, 'tp', axis=1, tiled=True)  36.7 us
    dot_general x2, matrix products, body(): jnp.einsum('bvk,bk->bv', mem_new, head_query, precision=lax.Precision.HIG...  17.2 us
    add x1, other arithmetic, body(): decay_own[:, None, None] * cell_memory[block_id]  10.4 us
    another operation x1, other arithmetic, body(): jnp.stack(memories)  8 us
  transfers between devices with their start and end apart: 4, of which 0 were waited for; matrix products, arithmetic and copies ran while one was open for 2% of the time, Pallas kernels for 0%

profile of v1, /device:TPU:0, one launch (start us, length us, event | category | flops | bytes accessed | tf_op | source)
XLA Modules:
  0.0 133.4 jit_solution(5327422206133025960)
XLA Ops:
  0.6 24.3 %all-gather = bf16[1280,128]{1,0:T(8,128)(2,1)S(1)} all-gather(bf16[80,128]{1,0:T(8,128)(2,1)} %param.17), channel_id=2, replica_groups=mesh['grp'=2,'tp'=16] {'tp'}, dimensions={0}, use_global_device_ids=true | all-gather | bytes 348160 | tf_op jit(solution)/shard_map/all_gather | solution.py:48
  25.2 0.7 convert_multiply_fusion
  25.8 0.8 slice_bitcast_fusion
  26.6 0.8 slice_convert_fusion
  27.4 0.8 slice_bitcast_fusion.1
  28.1 0.3 fusion.47
  28.4 1.3 fusion.38
  29.7 1.0 fusion.115
  30.7 1.0 multiply_reduce_fusion.5
  31.7 1.4 %fusion.103 = (f32[80,128]{1,0:T(8,128)S(1)}, bf16[80,128]{1,0:T(8,128)(2,1)S(1)}) fusion(f32[2,80,128]{2,1,0:T(8,128)} %param.20, f32[80]{0:T(128)S(1)} %get-tuple-element.6, f32[80]{0:T(128)S(1)} %get-tuple-element.7, bf16[2,2048,128]{2,1,0:T(8,128)(2,1)} %param.24, bf16[10,8,16,128]{3,2,1,0:T(8,128)(2,1)S(1)} %bitcast.191), kind=kOutput, calls=%fused_computation.137 | convolution fusion | flops 42004480 | bytes 955008 | tf_op jit(solution)/shard_map/dot_general | solution.py:62
  33.1 0.4 collective-permute-start
  33.7 1.3 fusion.37
  35.0 0.8 bitcast_convert_fusion
  36.0 8.7 %fusion.4 = f32[80,1,128]{2,1,0:T(1,128)S(1)} fusion(f32[2,80,128,256]{3,2,1,0:T(8,128)} %param.19, f32[80,256]{1,0:T(8,128)S(1)} %get-tuple-element.19, f32[80,128]{1,0:T(8,128)S(1)} %fusion.37, f32[80]{0:T(128)S(1)} %get-tuple-element.6, bf16[80,256,1]{1,0,2:T(8,128)(2,1)S(1)} %get-tuple-element.18), kind=kOutput, calls=%fused_computation.6 | convolution fusion | flops 39321600 | bytes 10690880 | tf_op jit(solution)/shard_map/bvk,bk->bv/dot_general | solution.py:108
  44.7 0.3 fusion.35
  44.9 18.3 %all_gather.20 = bf16[80,2048]{1,0:T(8,128)(2,1)S(1)} all-gather(bf16[80,128]{1,0:T(8,128)(2,1)S(1)} %fusion.35), channel_id=1, replica_groups=mesh['grp'=2,'tp'=16] {'tp'}, dimensions={1}, use_global_device_ids=true | all-gather | bytes 348160 | tf_op jit(solution)/shard_map/all_gather | solution.py:118
  63.3 0.2 fusion.17
  63.5 19.7 %all-gather.1 = bf16[1280,128]{1,0:T(8,128)(2,1)S(1)} all-gather(bf16[80,128]{1,0:T(8,128)(2,1)S(1)} %fusion.17), channel_id=3, replica_groups=mesh['grp'=2,'tp'=16] {'tp'}, dimensions={0}, use_global_device_ids=true | all-gather | bytes 348160 | tf_op jit(solution)/shard_map/all_gather | solution.py:48
  83.4 0.3 fusion.45
  83.7 0.2 fusion.39
  84.2 0.2 multiply_reduce_fusion.3
  84.4 0.2 fusion.28
  84.7 0.2 fusion.102
  85.0 0.4 collective-permute-start.2
  85.5 0.6 pad_maximum_fusion.1
  86.2 0.6 pad_maximum_fusion.6
  87.0 10.4 %multiply_add_fusion.1 = (f32[1,80,128,256]{3,2,1,0:T(8,128)S(1)}, f32[1,80,128,256]{3,2,1,0:T(8,128)S(1)}) fusion(f32[2,80,128,256]{3,2,1,0:T(8,128)} %param.19, f32[80,256]{1,0:T(8,128)S(1)} %get-tuple-element.19, f32[80,128]{1,0:T(8,128)S(1)} %fusion.37, f32[80]{0:T(128)S(1)} %get-tuple-element.6, f32[80,256]{1,0:T(8,128)S(1)} %get-tuple-element.13, ...), kind=kLoop, calls=%fused_computation.8 | loop fusion | flops 15728640 | bytes 42189440 | tf_op jit(solution)/shard_map/add | solution.py:103
  97.3 8.6 %fusion.1 = f32[80,1,128]{2,1,0:T(1,128)S(1)} fusion(f32[2,80,128,256]{3,2,1,0:T(8,128)} %param.19, f32[80,256]{1,0:T(8,128)S(1)} %get-tuple-element.13, f32[80,128]{1,0:T(8,128)S(1)} %fusion.28, f32[80]{0:T(128)S(1)} %get-tuple-element.4, bf16[80,256,1]{1,0,2:T(8,128)(2,1)S(1)} %get-tuple-element.12), kind=kOutput, calls=%fused_computation.3 | convolution fusion | flops 39321600 | bytes 10690880 | tf_op jit(solution)/shard_map/bvk,bk->bv/dot_general | solution.py:108
  105.9 0.3 fusion.26
  106.2 18.3 %all_gather.23 = bf16[80,2048]{1,0:T(8,128)(2,1)S(1)} all-gather(bf16[80,128]{1,0:T(8,128)(2,1)S(1)} %fusion.26), channel_id=1, replica_groups=mesh['grp'=2,'tp'=16] {'tp'}, dimensions={1}, use_global_device_ids=true | all-gather | bytes 348160 | tf_op jit(solution)/shard_map/all_gather | solution.py:118
  124.5 0.9 fusion.19
  125.4 8.0 %pad_maximum_fusion = f32[2,80,128,256]{3,2,1,0:T(8,128)} fusion(f32[1,80,128,256]{3,2,1,0:T(8,128)S(1)} %get-tuple-element.9, f32[1,80,128,256]{3,2,1,0:T(8,128)S(1)} %get-tuple-element.8), kind=kLoop, calls=%fused_computation | loop fusion | flops 5242880 | bytes 41943040 | tf_op jit(solution)/shard_map/stack | solution.py:126
  (46 shorter events, 1.3 us)
Async XLA Ops:
  25.1 38.2 %copy-start = (bf16[80,128]{1,0:T(8,128)(2,1)S(1)}, bf16[80,128]{1,0:T(8,128)(2,1)}, u32[]{:S(2)}) copy-start(bf16[80,128]{1,0:T(8,128)(2,1)} %param.17) | copy-start | bytes 61444
  31.7 52.0 %copy-start.1 = (bf16[2,2048,128]{2,1,0:T(8,128)(2,1)S(1)}, bf16[2,2048,128]{2,1,0:T(8,128)(2,1)}, u32[]{:S(2)}) copy-start(bf16[2,2048,128]{2,1,0:T(8,128)(2,1)} %param.23) | copy-start | bytes 3145732
  33.1 2.7 %collective-permute-start = (bf16[2,80,128]{2,1,0:T(8,128)(2,1)S(1)}, bf16[2,80,128]{2,1,0:T(8,128)(2,1)S(1)}, u32[]{:S(2)}, u32[]{:S(2)}) collective-permute-start(bf16[2,80,128]{2,1,0:T(8,128)(2,1)S(1)} %pad_maximum_fusion.4), channel_id=1, source_target_pairs={{0,1},{1,0},{2,3},{3,2},{4,5},{5,4},{6,7},{7,6},{8,9},{9,8},{10,11... | collective-permute-start | bytes 122888 | tf_op jit(solution)/shard_map/ppermute | solution.py:15
  33.5 50.5 %copy-start.7 = (bf16[2,2048,8]{1,2,0:T(8,128)(2,1)S(1)}, bf16[2,2048,8]{1,2,0:T(8,128)(2,1)}, u32[]{:S(2)}) copy-start(bf16[2,2048,8]{1,2,0:T(8,128)(2,1)} %param.28) | copy-start | bytes 196612
  33.5 50.5 %copy-start.9 = (f32[2,80,8]{1,2,0:T(8,128)S(1)}, f32[2,80,8]{1,2,0:T(8,128)}, u32[]{:S(2)}) copy-start(f32[2,80,8]{1,2,0:T(8,128)} %param.21) | copy-start | bytes 15364
  33.5 2.3 %collective-permute-start.1 = (f32[80,128]{1,0:T(8,128)S(1)}, f32[80,128]{1,0:T(8,128)S(1)}, u32[]{:S(2)}, u32[]{:S(2)}) collective-permute-start(f32[80,128]{1,0:T(8,128)S(1)} %get-tuple-element.34), channel_id=1, source_target_pairs={{0,1},{1,0},{2,3},{3,2},{4,5},{5,4},{6,7},{7,6},{8,9},{9,8},{10,11... | collective-permute-start | bytes 122888 | tf_op jit(solution)/shard_map/ppermute | solution.py:15
  34.9 49.2 %copy-start.8 = (bf16[2,2048,8]{1,2,0:T(8,128)(2,1)S(1)}, bf16[2,2048,8]{1,2,0:T(8,128)(2,1)}, u32[]{:S(2)}) copy-start(bf16[2,2048,8]{1,2,0:T(8,128)(2,1)} %param.27) | copy-start | bytes 196612
  35.0 49.5 %copy-start.2 = (bf16[2,2048,128]{2,1,0:T(8,128)(2,1)S(1)}, bf16[2,2048,128]{2,1,0:T(8,128)(2,1)}, u32[]{:S(2)}) copy-start(bf16[2,2048,128]{2,1,0:T(8,128)(2,1)} %param.25) | copy-start | bytes 3145732
  35.7 8.9 %copy-start.4 = (bf16[2,2048,128]{2,1,0:T(8,128)(2,1)S(1)}, bf16[2,2048,128]{2,1,0:T(8,128)(2,1)}, u32[]{:S(2)}) copy-start(bf16[2,2048,128]{2,1,0:T(8,128)(2,1)} %param.26) | copy-start | bytes 3145732
  35.7 27.5 %copy-start.5 = (bf16[2,2048,128]{2,1,0:T(8,128)(2,1)S(1)}, bf16[2,2048,128]{2,1,0:T(8,128)(2,1)}, u32[]{:S(2)}) copy-start(bf16[2,2048,128]{2,1,0:T(8,128)(2,1)} %param.33) | copy-start | bytes 3145732
  35.9 48.7 %copy-start.3 = (bf16[2,2048,128]{2,1,0:T(8,128)(2,1)S(1)}, bf16[2,2048,128]{2,1,0:T(8,128)(2,1)}, u32[]{:S(2)}) copy-start(bf16[2,2048,128]{2,1,0:T(8,128)(2,1)} %param.24) | copy-start | bytes 3145732
  35.9 48.7 %copy-start.6 = (f32[2,80,128]{2,1,0:T(8,128)S(1)}, f32[2,80,128]{2,1,0:T(8,128)}, u32[]{:S(2)}) copy-start(f32[2,80,128]{2,1,0:T(8,128)} %param.20) | copy-start | bytes 245764
  85.0 1.8 %collective-permute-start.2 = (bf16[2,80,128]{2,1,0:T(8,128)(2,1)S(1)}, bf16[2,80,128]{2,1,0:T(8,128)(2,1)S(1)}, u32[]{:S(2)}, u32[]{:S(2)}) collective-permute-start(bf16[2,80,128]{2,1,0:T(8,128)(2,1)S(1)} %pad_maximum_fusion.5), channel_id=1, source_target_pairs={{0,1},{1,0},{2,3},{3,2},{4,5},{5,4},{6,7},{7,6},{8,9},{9,8},{10,11... | collective-permute-start | bytes 122888 | tf_op jit(solution)/shard_map/ppermute | solution.py:15
  85.4 1.4 %collective-permute-start.3 = (f32[80,128]{1,0:T(8,128)S(1)}, f32[80,128]{1,0:T(8,128)S(1)}, u32[]{:S(2)}, u32[]{:S(2)}) collective-permute-start(f32[80,128]{1,0:T(8,128)S(1)} %get-tuple-element.36), channel_id=1, source_target_pairs={{0,1},{1,0},{2,3},{3,2},{4,5},{5,4},{6,7},{7,6},{8,9},{9,8},{10,11... | collective-permute-start | bytes 122888 | tf_op jit(solution)/shard_map/ppermute | solution.py:15
